TPU v7x, 32 devices: a whole 2x2x4 slice. The times are simulated.
32 devices in a mesh: sp: 8 (over z, y), tp: 4 (over x, core).
Axes of the slice: x: 2, y: 2, z: 4, core: 2. Of those that a mesh axis runs over, the one named last changes fastest.
Arguments:
- queries: bfloat16 [3072, 2048], P('sp', 'tp'), may hold values from -200 to 200
- keys: bfloat16 [3072, 2048], P('sp', 'tp'), may hold values from -200 to 200
- values: bfloat16 [3072, 2048], P('sp', 'tp'), may hold values from -6 to 6
- forget_sums: float32 [3072, 16], P('sp', 'tp'), may hold values from -3072 to 0, as said below
- residual_in: bfloat16 [3072, 2048], P(('sp', 'tp')), may hold values from -0.59765625 to 0.59765625
- out_weight: bfloat16 [2048, 2048], P('tp'), may hold values from -0.125 to 0.125
- norm_gain: bfloat16 [2048], replicated, may hold values from 0.099609375 to 1.8984375
- gate_weight: bfloat16 [2048, 3072], P('sp', 'tp'), may hold values from -0.125 to 0.125
- up_weight: bfloat16 [2048, 3072], P('sp', 'tp'), may hold values from -0.125 to 0.125
- down_weight: bfloat16 [3072, 2048], P('tp', 'sp'), may hold values from -0.109375 to 0.109375
Outputs:
- mixed: bfloat16 [3072, 2048], P(('sp', 'tp'))
Inputs may be any that keep to these rules, and one draw needn't show every extreme that they name: `forget_sums`: in every head the entries never rise from one position to the next.
All inputs are finite; a program needn't handle non-finite values.
Results may differ from a plain program's by a relative error of at most 0.022.
Values may be sent and summed in bfloat16 or wider, within the bound.
A program may use at most 192 MiB of HBM per device.

v0:
```python
import math
import jax
import jax.numpy as jnp
from jax import lax
from jax.sharding import PartitionSpec as P

HD = 128


def attend_block(carried, block, query_rows, query_gate, query_pos, heads_here):
    row_top, row_total, weighted = carried
    key_rows, value_rows, key_gate, key_pos = block
    score_scale = HD ** (-0.5)
    tops, totals, sums = ([], [], [])
    for head_index in range(heads_here):
        columns = slice(head_index * HD, (head_index + 1) * HD)
        scores = (
            jnp.einsum(
                "qd,kd->qk",
                query_rows[:, columns],
                key_rows[:, columns],
                preferred_element_type=jnp.float32,
            )
            * score_scale
        )
        scores = scores + query_gate[:, head_index : head_index + 1] - key_gate[None, :, head_index]
        scores = jnp.where(key_pos[None, :] <= query_pos[:, None], scores, -jnp.inf)
        new_top = jnp.maximum(row_top[:, head_index], jnp.max(scores, axis=1))
        shrink = jnp.exp(row_top[:, head_index] - new_top)
        expon = jnp.exp(scores - new_top[:, None])
        totals.append(shrink * row_total[:, head_index] + jnp.sum(expon, axis=1))
        sums.append(
            shrink[:, None] * weighted[:, columns]
            + jnp.dot(
                expon.astype(jnp.bfloat16),
                value_rows[:, columns],
                preferred_element_type=jnp.float32,
            )
        )
        tops.append(new_top)
    return (jnp.stack(tops, axis=1), jnp.stack(totals, axis=1), jnp.concatenate(sums, axis=1))


def shards(
    queries,
    keys,
    values,
    forget_sums,
    residual_in,
    out_weight,
    norm_gain,
    gate_weight,
    up_weight,
    down_weight,
):
    rows_here = queries.shape[0]
    heads_here = queries.shape[1] // HD
    first = lax.axis_index("sp") * rows_here
    query_pos = first + jnp.arange(rows_here, dtype=jnp.int32)
    early_gate, early_up = (
        lax.all_gather(gate_weight, "sp", axis=0, tiled=True),
        lax.all_gather(up_weight, "sp", axis=0, tiled=True),
    )
    all_gates = lax.all_gather(forget_sums, "sp", axis=0, tiled=True)
    start_state = (
        jnp.full((rows_here, heads_here), -1e30, jnp.float32),
        jnp.zeros((rows_here, heads_here), jnp.float32),
        jnp.zeros((rows_here, heads_here * HD), jnp.float32),
    )
    carried = start_state
    key_rows = lax.all_gather(keys, "sp", axis=0, tiled=True)
    value_rows = lax.all_gather(values, "sp", axis=0, tiled=True)
    count = key_rows.shape[0]
    block_rows = math.gcd(count, 512)
    block_count = count // block_rows
    key_pos = jnp.arange(count, dtype=jnp.int32)
    blocks = (
        key_rows.reshape(block_count, block_rows, -1),
        value_rows.reshape(block_count, block_rows, -1),
        all_gates.reshape(block_count, block_rows, -1),
        key_pos.reshape(block_count, block_rows),
    )

    def advance(inner, block):
        return (attend_block(inner, block, queries, forget_sums, query_pos, heads_here), None)

    carried, unused = lax.scan(advance, carried, blocks)
    row_top, row_total, weighted = carried
    attended = (weighted / jnp.repeat(row_total, HD, axis=1)).astype(jnp.bfloat16)
    projected = lax.psum_scatter(
        jnp.dot(attended, out_weight, preferred_element_type=jnp.float32).astype(jnp.bfloat16),
        "tp",
        scatter_dimension=0,
        tiled=True,
    ).astype(jnp.float32)
    stream = residual_in.astype(jnp.float32) + projected
    normed = stream * lax.rsqrt(jnp.mean(stream * stream, axis=1, keepdims=True) + 1e-06)
    normed = (normed * norm_gain.astype(jnp.float32)).astype(jnp.bfloat16)
    every_row = lax.all_gather(normed, "tp", axis=0, tiled=True)
    gate = jnp.dot(every_row, early_gate, preferred_element_type=jnp.float32)
    up = jnp.dot(every_row, early_up, preferred_element_type=jnp.float32)
    hidden = (jax.nn.silu(gate) * up).astype(jnp.bfloat16)
    partial_value = jnp.dot(
        hidden,
        lax.all_gather(down_weight, "sp", axis=1, tiled=True),
        preferred_element_type=jnp.float32,
    ).astype(jnp.bfloat16)
    summed = lax.psum_scatter(
        partial_value.astype(jnp.float32).astype(jnp.bfloat16),
        "tp",
        scatter_dimension=0,
        tiled=True,
    ).astype(jnp.float32)
    return (stream + summed).astype(jnp.bfloat16)


def solution(mesh):
    placed = (
        P("sp", "tp"),
        P("sp", "tp"),
        P("sp", "tp"),
        P("sp", "tp"),
        P(("sp", "tp"), None),
        P("tp", None),
        P(),
        P("sp", "tp"),
        P("sp", "tp"),
        P("tp", "sp"),
    )
    return jax.shard_map(
        shards, mesh=mesh, in_specs=placed, out_specs=P(("sp", "tp"), None), check_vma=False
    )
```

profile of v0, /device:TPU:0, one launch (start us, length us, event | category | flops | bytes accessed | tf_op | source)
XLA Modules:
  0.0 441.7 jit_solution(3732854181924096891)
XLA Ops:
  6.5 0.7 all-gather.7.cloned.1.call-update
  7.3 0.7 all-gather.9.cloned.1.call-update
  8.1 32.9 %all_gather.22 = f32[3072,4]{0,1:T(4,128)S(1)} all-gather(f32[384,4]{0,1:T(4,128)} %param.15), channel_id=1, replica_groups=mesh['sp'=8,'tp'=4] {'sp'}, dimensions={0}, use_global_device_ids=true | all-gather | bytes 55296 | tf_op jit(solution)/shard_map/all_gather | solution.py:64
  41.0 31.5 %all-gather.7.cloned.1.call-done = bf16[3072,512]{1,0:T(8,128)(2,1)} async-done(((bf16[384,512]{1,0:T(8,128)(2,1)}), bf16[3072,512]{1,0:T(8,128)(2,1)}) %all-gather.7.cloned.1.call-update) | async-done | bytes 3145744 | tf_op jit(solution)/shard_map/all_gather | solution.py:71
  72.5 60.9 %all-gather.9.cloned.1.call-done = bf16[3072,512]{1,0:T(8,128)(2,1)} async-done(((bf16[384,512]{1,0:T(8,128)(2,1)}), bf16[3072,512]{1,0:T(8,128)(2,1)}) %all-gather.9.cloned.1.call-update) | async-done | bytes 3145744 | tf_op jit(solution)/shard_map/all_gather | solution.py:72
  133.5 28.8 %while.15 = (s32[]{:T(128)}, f32[384,4]{0,1:T(4,128)S(1)}, f32[384,4]{0,1:T(4,128)S(1)}, f32[384,512]{0,1:T(8,128)S(1)}, s32[6,512]{1,0:T(8,128)S(1)}, /*index=5...) while((s32[]{:T(128)}, f32[384,4]{0,1:T(4,128)S(1)}, ...), condition=%wide.region_9.10_spmd.clone, body=%wide.region_0.9_spmd.clone.sunk | while | flops 411514752 | bytes 16326277 | solution.py:87
  133.5 1.3 dynamic-slice_bitcast_fusion.6
  135.6 0.4 fusion.92
  138.3 1.3 dynamic-slice_bitcast_fusion.6
  139.7 0.3 fusion.90
  143.1 1.3 dynamic-slice_bitcast_fusion.6
  144.5 0.3 fusion.90
  147.9 1.3 dynamic-slice_bitcast_fusion.6
  149.3 0.3 fusion.90
  152.7 1.3 dynamic-slice_bitcast_fusion.6
  154.1 0.3 fusion.90
  157.5 1.3 dynamic-slice_bitcast_fusion.6
  162.4 2.2 convolution_convert_fusion.1
  164.6 0.5 all-gather.13.cloned.1.call-update
  165.2 26.2 %reduce-scatter.3.cloned.1.call-done = bf16[96,2048]{1,0:T(8,128)(2,1)} async-done(((bf16[384,2048]{1,0:T(8,128)(2,1)}), bf16[96,2048]{1,0:T(8,128)(2,1)}) %reduce-scatter.3.cloned.1.call-update) | async-done | bytes 393232 | tf_op jit(solution)/shard_map/reduce_scatter | solution.py:90
  191.4 1.2 multiply_reduce_fusion
  192.7 1.9 multiply_convert_fusion
  194.7 0.5 all-gather.15.cloned.1.call-update
  195.2 0.7 all-gather.17.cloned.1.call-update
  196.0 57.5 %all-gather.13.cloned.1.call-done = bf16[2048,768]{1,0:T(8,128)(2,1)} async-done(((bf16[256,768]{1,0:T(8,128)(2,1)}), bf16[2048,768]{1,0:T(8,128)(2,1)}) %all-gather.13.cloned.1.call-update) | async-done | bytes 3145744 | tf_op jit(solution)/shard_map/all_gather | solution.py:61
  253.5 19.7 %all-gather.11.cloned.1.call-done = bf16[384,2048]{1,0:T(8,128)(2,1)} async-done(((bf16[96,2048]{1,0:T(8,128)(2,1)}), bf16[384,2048]{1,0:T(8,128)(2,1)}) %all-gather.11.cloned.1.call-update) | async-done | bytes 1572880 | tf_op jit(solution)/shard_map/all_gather | solution.py:99
  273.3 4.8 %fusion.55 = f32[384,768]{1,0:T(8,128)} fusion(bf16[384,2048]{1,0:T(8,128)(2,1)} %all-gather.11.cloned.1.call-done, bf16[2048,768]{1,0:T(8,128)(2,1)} %all-gather.13.cloned.1.call-done), kind=kOutput, calls=%fused_computation.100 | convolution fusion | flops 1207959552 | bytes 5898240 | tf_op jit(solution)/shard_map/dot_general | solution.py:100
  278.0 57.3 %all-gather.15.cloned.1.call-done = bf16[2048,768]{1,0:T(8,128)(2,1)} async-done(((bf16[256,768]{1,0:T(8,128)(2,1)}), bf16[2048,768]{1,0:T(8,128)(2,1)}) %all-gather.15.cloned.1.call-update) | async-done | bytes 3145744 | tf_op jit(solution)/shard_map/all_gather | solution.py:62
  335.4 63.4 %all-gather.17.cloned.1.call-done = bf16[768,2048]{1,0:T(8,128)(2,1)} async-done(((bf16[768,256]{1,0:T(8,128)(2,1)}), bf16[768,2048]{1,0:T(8,128)(2,1)}) %all-gather.17.cloned.1.call-update) | async-done | bytes 3145744 | tf_op jit(solution)/shard_map/all_gather | solution.py:105
  398.7 7.9 %convolution_convert_fusion = bf16[384,2048]{1,0:T(8,128)(2,1)} fusion(bf16[768,2048]{1,0:T(8,128)(2,1)} %all-gather.17.cloned.1.call-done, bf16[384,2048]{1,0:T(8,128)(2,1)} %all-gather.11.cloned.1.call-done, bf16[2048,768]{1,0:T(8,128)(2,1)} %all-gather.15.cloned.1.call-done, f32[384,768]{1,0:T(8,128)} %fusion.55), kind=kOutput, calls=%fused_computation.81 | convolution fusion | flops 2418475008 | bytes 10616832 | tf_op jit(solution)/shard_map/dot_general | solution.py:103
  406.6 26.4 %reduce-scatter.5.cloned.1.call-done = bf16[96,2048]{1,0:T(8,128)(2,1)} async-done(((bf16[384,2048]{1,0:T(8,128)(2,1)}), bf16[96,2048]{1,0:T(8,128)(2,1)}) %reduce-scatter.5.cloned.1.call-update) | async-done | bytes 393232 | tf_op jit(solution)/shard_map/reduce_scatter | solution.py:108
  433.0 1.9 add_convert_fusion
  (157 shorter events, 19.2 us)
Async XLA Ops:
  6.5 155.8 %copy-start = (bf16[512,2048]{1,0:T(8,128)(2,1)S(1)}, bf16[512,2048]{1,0:T(8,128)(2,1)}, u32[]{:S(2)}) copy-start(bf16[512,2048]{1,0:T(8,128)(2,1)} %param.17) | copy-start | bytes 6291460
  6.5 126.9 %copy-start.3 = (f32[384,4]{0,1:T(4,128)S(1)}, f32[384,4]{0,1:T(4,128)}, u32[]{:S(2)}) copy-start(f32[384,4]{0,1:T(4,128)} %param.15) | copy-start | bytes 18436
  6.5 126.9 %copy-start.5 = (bf16[384,512]{1,0:T(8,128)(2,1)S(1)}, bf16[384,512]{1,0:T(8,128)(2,1)}, u32[]{:S(2)}) copy-start(bf16[384,512]{1,0:T(8,128)(2,1)} %param.12) | copy-start | bytes 1179652
  6.5 65.9 %all-gather.7.cloned.1.call-start = ((), (), s32[]{:S(2)}) async-start(), calls=%async_computation.2 | async-start | bytes 3538944 | tf_op jit(solution)/shard_map/all_gather | solution.py:71
  7.3 126.1 %all-gather.9.cloned.1.call-start = ((), (), s32[]{:S(2)}) async-start(), calls=%async_computation.3 | async-start | bytes 3538944 | tf_op jit(solution)/shard_map/all_gather | solution.py:72
  8.0 183.4 %reduce-scatter.3.cloned.1.call-start = ((), (), s32[]{:S(2)}) async-start(), calls=%async_computation.4 | async-start | bytes 1966080 | tf_op jit(solution)/shard_map/reduce_scatter | solution.py:90
  164.5 0.7 copy-start.4
  164.5 26.9 %copy-start.1 = (bf16[96,2048]{1,0:T(8,128)(2,1)S(1)}, bf16[96,2048]{1,0:T(8,128)(2,1)}, u32[]{:S(2)}) copy-start(bf16[96,2048]{1,0:T(8,128)(2,1)} %param.16) | copy-start | bytes 1179652
  164.6 89.0 %all-gather.13.cloned.1.call-start = ((), (), s32[]{:S(2)}) async-start(), calls=%async_computation.6 | async-start | bytes 3538944 | tf_op jit(solution)/shard_map/all_gather | solution.py:61
  165.1 108.1 %all-gather.11.cloned.1.call-start = ((), (), s32[]{:S(2)}) async-start(), calls=%async_computation.5 | async-start | bytes 1966080 | tf_op jit(solution)/shard_map/all_gather | solution.py:99
  194.6 140.7 %all-gather.15.cloned.1.call-start = ((), (), s32[]{:S(2)}) async-start(), calls=%async_computation.7 | async-start | bytes 3538944 | tf_op jit(solution)/shard_map/all_gather | solution.py:62
  195.2 203.6 %all-gather.17.cloned.1.call-start = ((), (), s32[]{:S(2)}) async-start(), calls=%async_computation.8 | async-start | bytes 3538944 | tf_op jit(solution)/shard_map/all_gather | solution.py:105
  195.9 237.1 %reduce-scatter.5.cloned.1.call-start = ((), (), s32[]{:S(2)}) async-start(), calls=%async_computation.9 | async-start | bytes 1966080 | tf_op jit(solution)/shard_map/reduce_scatter | solution.py:108
  406.6 26.4 %copy-start.2 = (bf16[96,2048]{1,0:T(8,128)(2,1)S(1)}, bf16[96,2048]{1,0:T(8,128)(2,1)}, u32[]{:S(2)}) copy-start(bf16[96,2048]{1,0:T(8,128)(2,1)} %reduce-scatter.3.cloned.1.call-done) | copy-start | bytes 1179652
Sparse Core Ops, SparseCore 0:
  9.5 62.9 all-gather.6
  74.7 58.6 all-gather.8
  164.7 26.6 reduce-scatter.2
  193.5 60.0 all-gather.12
  254.9 18.2 all-gather.10
  275.3 60.0 all-gather.14
  337.4 61.2 all-gather.16
  406.7 26.2 reduce-scatter.4
where the time goes:
time: 442 us
  waiting for transfers between devices  346 us (78%)
  blocking collectives  32.9 us (7%)
  matrix products  30.1 us (7%)
  between operations  13.6 us (3%)
  other arithmetic  9.88 us (2%)
  local copies, waits for them, and re-layouts  8.11 us (2%)
    all_gather x1, waiting for transfers between devices, shards(): lax.all_gather(down_weight, 'sp', axis=1, tiled=True)  63.4 us
    all_gather x1, waiting for transfers between devices, shards(): value_rows = lax.all_gather(values, 'sp', axis=0, tiled=True)  60.9 us
    all_gather x1, waiting for transfers between devices, shards(): lax.all_gather(gate_weight, 'sp', axis=0, tiled=True)  57.5 us
    all_gather x1, waiting for transfers between devices, shards(): lax.all_gather(up_weight, 'sp', axis=0, tiled=True)  57.3 us
    all_gather x1, blocking collectives, shards(): all_gates = lax.all_gather(forget_sums, 'sp', axis=0, tiled=True)  32.9 us
    all_gather x1, waiting for transfers between devices, shards(): key_rows = lax.all_gather(keys, 'sp', axis=0, tiled=True)  31.5 us
    reduce_scatter x1, waiting for transfers between devices, shards(): lax.psum_scatter(partial_value.astype(jnp.float32).astype(jnp.bfloat16),...  26.4 us
    reduce_scatter x1, waiting for transfers between devices, shards(): lax.psum_scatter(jnp.dot(attended, out_weight, preferred_element_type=jnp...  26.2 us
  transfers between devices with their start and end apart: 8, of which 8 were waited for; matrix products, arithmetic and copies ran while one was open for 2% of the time, Pallas kernels for 0%

commit v1 on v0

--- a/solution.py
+++ b/solution.py
@@ -61,14 +61,17 @@
         lax.all_gather(gate_weight, "sp", axis=0, tiled=True),
         lax.all_gather(up_weight, "sp", axis=0, tiled=True),
     )
-    all_gates = lax.all_gather(forget_sums, "sp", axis=0, tiled=True)
     start_state = (
         jnp.full((rows_here, heads_here), -1e30, jnp.float32),
         jnp.zeros((rows_here, heads_here), jnp.float32),
         jnp.zeros((rows_here, heads_here * HD), jnp.float32),
     )
     carried = start_state
-    key_rows = lax.all_gather(keys, "sp", axis=0, tiled=True)
+    all_gates, key_rows = jnp.split(
+        lax.all_gather(jnp.concatenate([forget_sums, keys], axis=1), "sp", axis=0, tiled=True),
+        [forget_sums.shape[1]],
+        axis=1,
+    )
     value_rows = lax.all_gather(values, "sp", axis=0, tiled=True)
     count = key_rows.shape[0]
     block_rows = math.gcd(count, 512)

time: 442 us -> 500 us (1.13)
  waiting for transfers between devices: 346 us -> 423 us
  blocking collectives: 32.9 us -> 0 us
  local copies, waits for them, and re-layouts: 8.11 us -> 19.8 us
    all_gather x1, waiting for transfers between devices: 31.5 us -> 120 us  [shards(): lax.all_gather(jnp.concatenate([forget_sums, keys], axis=1), 'sp', axis=0...]
    all_gather x1 -> x0, blocking collectives: 32.9 us -> none  [shards(): all_gates = lax.all_gather(forget_sums, 'sp', axis=0, tiled=True)]
    all_gather x1, waiting for transfers between devices: 60.9 us -> 49.6 us  [shards(): value_rows = lax.all_gather(values, 'sp', axis=0, tiled=True)]
    split x0 -> x2, local copies, waits for them, and re-layouts: none -> 8.92 us  [shards(): jnp.split(lax.all_gather(jnp.concatenate([forget_sums, keys], axis=1), 's...]
  transfers between devices with their start and end apart: 8 -> 8, of which waited for: 8 -> 8; matrix products, arithmetic and copies ran while one was open for 2% -> 4% of each run, Pallas kernels for 0% -> 0%
where the time goes in v1:
time: 500 us; the launch traced here: 499 us
  waiting for transfers between devices  423 us (85%)
  matrix products  30.1 us (6%)
  local copies, waits for them, and re-layouts  19.8 us (4%)
  between operations  13.6 us (3%)
  other arithmetic  12.4 us (2%)
    all_gather x1, waiting for transfers between devices, shards(): lax.all_gather(jnp.concatenate([forget_sums, keys], axis=1), 'sp', axis=0...  120 us
    all_gather x1, waiting for transfers between devices, shards(): lax.all_gather(down_weight, 'sp', axis=1, tiled=True)  63.4 us
    all_gather x1, waiting for transfers between devices, shards(): lax.all_gather(gate_weight, 'sp', axis=0, tiled=True)  57.6 us
    all_gather x1, waiting for transfers between devices, shards(): lax.all_gather(up_weight, 'sp', axis=0, tiled=True)  57.3 us
    all_gather x1, waiting for transfers between devices, shards(): value_rows = lax.all_gather(values, 'sp', axis=0, tiled=True)  49.6 us
    reduce_scatter x1, waiting for transfers between devices, shards(): lax.psum_scatter(partial_value.astype(jnp.float32).astype(jnp.bfloat16),...  26.4 us
    reduce_scatter x1, waiting for transfers between devices, shards(): lax.psum_scatter(jnp.dot(attended, out_weight, preferred_element_type=jnp...  26.1 us
    all_gather x1, waiting for transfers between devices, shards(): every_row = lax.all_gather(normed, 'tp', axis=0, tiled=True)  19.7 us
  transfers between devices with their start and end apart: 8, of which 8 were waited for; matrix products, arithmetic and copies ran while one was open for 4% of the time, Pallas kernels for 0%

profile of v1, /device:TPU:0, one launch (start us, length us, event | category | flops | bytes accessed | tf_op | source)
XLA Modules:
  0.0 499.4 jit_solution(13620481617680688380)
XLA Ops:
  6.5 1.2 convert_element_type.48
  7.8 0.8 copy.12
  8.6 1.3 pad_maximum_fusion.3
  10.0 0.7 all-gather.9.cloned.1.call-update
  10.7 120.0 %all-gather.7.cloned.1.call-done = f32[3072,516]{1,0:T(8,128)} async-done(((f32[384,516]{1,0:T(8,128)}), f32[3072,516]{1,0:T(8,128)}) %all-gather.7.cloned.1.call-update) | async-done | bytes 6340624 | tf_op jit(solution)/shard_map/all_gather | solution.py:71
  130.7 2.6 split.9
  133.4 1.9 copy.14
  135.3 6.3 %split.8 = bf16[3072,512]{1,0:T(8,128)(2,1)} slice(f32[3072,516]{1,0:T(8,128)} %all-gather.7.cloned.1.call-done), slice={[0:3072], [4:516]} | slice | bytes 6291456 | tf_op jit(solution)/shard_map/split | solution.py:70
  141.5 49.6 %all-gather.9.cloned.1.call-done = bf16[3072,512]{1,0:T(8,128)(2,1)} async-done(((bf16[384,512]{1,0:T(8,128)(2,1)}), bf16[3072,512]{1,0:T(8,128)(2,1)}) %all-gather.9.cloned.1.call-update) | async-done | bytes 3145744 | tf_op jit(solution)/shard_map/all_gather | solution.py:75
  191.2 28.8 %while.15 = (s32[]{:T(128)}, f32[384,4]{0,1:T(4,128)S(1)}, f32[384,4]{0,1:T(4,128)S(1)}, f32[384,512]{0,1:T(8,128)S(1)}, s32[6,512]{1,0:T(8,128)S(1)}, /*index=5...) while((s32[]{:T(128)}, f32[384,4]{0,1:T(4,128)S(1)}, ...), condition=%wide.region_9.10_spmd.clone, body=%wide.region_0.9_spmd.clone.sunk | while | flops 411514752 | bytes 16326277 | solution.py:90
  191.2 1.3 dynamic-slice_bitcast_fusion.6
  196.0 1.3 dynamic-slice_bitcast_fusion.6
  200.9 1.3 dynamic-slice_bitcast_fusion.6
  202.2 0.3 fusion.90
  205.7 1.3 dynamic-slice_bitcast_fusion.6
  210.5 1.3 dynamic-slice_bitcast_fusion.6
  215.3 1.3 dynamic-slice_bitcast_fusion.6
  220.1 2.2 convolution_convert_fusion.1
  222.4 0.5 all-gather.13.cloned.1.call-update
  223.0 26.1 %reduce-scatter.3.cloned.1.call-done = bf16[96,2048]{1,0:T(8,128)(2,1)} async-done(((bf16[384,2048]{1,0:T(8,128)(2,1)}), bf16[96,2048]{1,0:T(8,128)(2,1)}) %reduce-scatter.3.cloned.1.call-update) | async-done | bytes 393232 | tf_op jit(solution)/shard_map/reduce_scatter | solution.py:93
  249.1 1.2 multiply_reduce_fusion
  250.4 1.9 multiply_convert_fusion
  252.3 0.5 all-gather.15.cloned.1.call-update
  252.9 0.7 all-gather.17.cloned.1.call-update
  253.7 57.6 %all-gather.13.cloned.1.call-done = bf16[2048,768]{1,0:T(8,128)(2,1)} async-done(((bf16[256,768]{1,0:T(8,128)(2,1)}), bf16[2048,768]{1,0:T(8,128)(2,1)}) %all-gather.13.cloned.1.call-update) | async-done | bytes 3145744 | tf_op jit(solution)/shard_map/all_gather | solution.py:61
  311.2 19.7 %all-gather.11.cloned.1.call-done = bf16[384,2048]{1,0:T(8,128)(2,1)} async-done(((bf16[96,2048]{1,0:T(8,128)(2,1)}), bf16[384,2048]{1,0:T(8,128)(2,1)}) %all-gather.11.cloned.1.call-update) | async-done | bytes 1572880 | tf_op jit(solution)/shard_map/all_gather | solution.py:102
  331.0 4.8 fusion.55
  335.7 57.3 %all-gather.15.cloned.1.call-done = bf16[2048,768]{1,0:T(8,128)(2,1)} async-done(((bf16[256,768]{1,0:T(8,128)(2,1)}), bf16[2048,768]{1,0:T(8,128)(2,1)}) %all-gather.15.cloned.1.call-update) | async-done | bytes 3145744 | tf_op jit(solution)/shard_map/all_gather | solution.py:62
  393.0 63.4 %all-gather.17.cloned.1.call-done = bf16[768,2048]{1,0:T(8,128)(2,1)} async-done(((bf16[768,256]{1,0:T(8,128)(2,1)}), bf16[768,2048]{1,0:T(8,128)(2,1)}) %all-gather.17.cloned.1.call-update) | async-done | bytes 3145744 | tf_op jit(solution)/shard_map/all_gather | solution.py:108
  456.4 7.9 %convolution_convert_fusion = bf16[384,2048]{1,0:T(8,128)(2,1)} fusion(bf16[768,2048]{1,0:T(8,128)(2,1)} %all-gather.17.cloned.1.call-done, bf16[384,2048]{1,0:T(8,128)(2,1)} %all-gather.11.cloned.1.call-done, bf16[2048,768]{1,0:T(8,128)(2,1)} %all-gather.15.cloned.1.call-done, f32[384,768]{1,0:T(8,128)} %fusion.55), kind=kOutput, calls=%fused_computation.81 | convolution fusion | flops 2418475008 | bytes 10616832 | tf_op jit(solution)/shard_map/dot_general | solution.py:106
  464.3 26.4 %reduce-scatter.5.cloned.1.call-done = bf16[96,2048]{1,0:T(8,128)(2,1)} async-done(((bf16[384,2048]{1,0:T(8,128)(2,1)}), bf16[96,2048]{1,0:T(8,128)(2,1)}) %reduce-scatter.5.cloned.1.call-update) | async-done | bytes 393232 | tf_op jit(solution)/shard_map/reduce_scatter | solution.py:111
  490.7 1.9 add_convert_fusion
  (162 shorter events, 20.7 us)
Async XLA Ops:
  6.5 213.6 %copy-start = (bf16[512,2048]{1,0:T(8,128)(2,1)S(1)}, bf16[512,2048]{1,0:T(8,128)(2,1)}, u32[]{:S(2)}) copy-start(bf16[512,2048]{1,0:T(8,128)(2,1)} %param.17) | copy-start | bytes 6291460
  6.5 124.2 %all-gather.7.cloned.1.call-start = ((), (), s32[]{:S(2)}) async-start(), calls=%async_computation.2 | async-start | bytes 8847360 | tf_op jit(solution)/shard_map/all_gather | solution.py:71
  9.9 181.2 %all-gather.9.cloned.1.call-start = ((), (), s32[]{:S(2)}) async-start(), calls=%async_computation.3 | async-start | bytes 3538944 | tf_op jit(solution)/shard_map/all_gather | solution.py:75
  10.7 238.4 %reduce-scatter.3.cloned.1.call-start = ((), (), s32[]{:S(2)}) async-start(), calls=%async_computation.4 | async-start | bytes 1966080 | tf_op jit(solution)/shard_map/reduce_scatter | solution.py:93
  135.3 56.0 %copy-start.3 = (f32[384,4]{0,1:T(4,128)S(1)}, f32[384,4]{0,1:T(4,128)}, u32[]{:S(2)}) copy-start(f32[384,4]{0,1:T(4,128)} %param.15) | copy-start | bytes 18436
  135.3 56.0 %copy-start.5 = (bf16[384,512]{1,0:T(8,128)(2,1)S(1)}, bf16[384,512]{1,0:T(8,128)(2,1)}, u32[]{:S(2)}) copy-start(bf16[384,512]{1,0:T(8,128)(2,1)} %param.12) | copy-start | bytes 1179652
  222.3 0.7 copy-start.4
  222.3 26.8 %copy-start.1 = (bf16[96,2048]{1,0:T(8,128)(2,1)S(1)}, bf16[96,2048]{1,0:T(8,128)(2,1)}, u32[]{:S(2)}) copy-start(bf16[96,2048]{1,0:T(8,128)(2,1)} %param.16) | copy-start | bytes 1179652
  222.3 88.9 %all-gather.13.cloned.1.call-start = ((), (), s32[]{:S(2)}) async-start(), calls=%async_computation.6 | async-start | bytes 3538944 | tf_op jit(solution)/shard_map/all_gather | solution.py:61
  222.9 108.1 %all-gather.11.cloned.1.call-start = ((), (), s32[]{:S(2)}) async-start(), calls=%async_computation.5 | async-start | bytes 1966080 | tf_op jit(solution)/shard_map/all_gather | solution.py:102
  252.3 140.8 %all-gather.15.cloned.1.call-start = ((), (), s32[]{:S(2)}) async-start(), calls=%async_computation.7 | async-start | bytes 3538944 | tf_op jit(solution)/shard_map/all_gather | solution.py:62
  252.9 203.6 %all-gather.17.cloned.1.call-start = ((), (), s32[]{:S(2)}) async-start(), calls=%async_computation.8 | async-start | bytes 3538944 | tf_op jit(solution)/shard_map/all_gather | solution.py:108
  253.6 237.1 %reduce-scatter.5.cloned.1.call-start = ((), (), s32[]{:S(2)}) async-start(), calls=%async_computation.9 | async-start | bytes 1966080 | tf_op jit(solution)/shard_map/reduce_scatter | solution.py:111
  464.3 26.4 %copy-start.2 = (bf16[96,2048]{1,0:T(8,128)(2,1)S(1)}, bf16[96,2048]{1,0:T(8,128)(2,1)}, u32[]{:S(2)}) copy-start(bf16[96,2048]{1,0:T(8,128)(2,1)} %reduce-scatter.3.cloned.1.call-done) | copy-start | bytes 1179652
Sparse Core Ops, SparseCore 0:
  10.0 120.6 all-gather.6
  132.9 58.1 all-gather.8
  222.4 26.6 reduce-scatter.2
  251.2 60.0 all-gather.12
  312.6 18.2 all-gather.10
  333.0 60.0 all-gather.14
  395.1 61.2 all-gather.16
  464.4 26.2 reduce-scatter.4
